TPU v7x, 32 devices: a whole 2x2x4 slice. The times are simulated.
32 devices in a mesh: sp: 8 (over z, y), fs: 2 (over x), tp: 2 (over core).
Axes of the slice: x: 2, y: 2, z: 4, core: 2. Of those that a mesh axis runs over, the one named last changes fastest.
Arguments:
- ret_query: bfloat16 [1024, 2, 512], P('sp', 'fs', 'tp'), may hold values from -6 to 6
- ret_key: bfloat16 [1024, 2, 512], P('sp', 'fs', 'tp'), may hold values from -6 to 6
- ret_value: bfloat16 [1024, 2, 1024], P('sp', 'fs', 'tp'), may hold values from -6 to 6
- log_decay: float32 [2, 4, 1024], P('fs', 'tp', 'sp'), may hold values from -1.2 to 0
- ret_gain: float32 [1024], P('tp'), may hold values from 0.1 to 1.9
- mla_query: bfloat16 [1024, 2, 1536], P('sp', 'fs', 'tp'), may hold values from -64 to 64
- kv_latent: bfloat16 [1024, 2, 256], P('sp', 'fs'), may hold values from -6 to 6
- rope_key: bfloat16 [1024, 2, 64], P('sp', 'fs'), may hold values from -8 to 8
- key_up: bfloat16 [256, 1024], replicated, may hold values from -0.375 to 0.375
- value_up: bfloat16 [256, 1024], replicated, may hold values from -3 to 3
- ret_out: bfloat16 [1024, 2048], P('tp', 'fs'), may hold values from -0.1875 to 0.1875
- mla_out: bfloat16 [1024, 2048], P('tp', 'fs'), may hold values from -0.1875 to 0.1875
Outputs:
- mixed_rows: bfloat16 [1024, 2, 2048], P(('sp', 'tp'), 'fs')
- log_weight: float32 [2, 8, 1024], P('fs', 'tp', 'sp')
All inputs are finite; a program needn't handle non-finite values.
Results may differ from a plain program's by a relative error of at most 0.014.
Values may be sent and summed in bfloat16 or wider, within the bound.
No kernel may reach another device: no remote copies, remote signals or barrier semaphores. Data moves between devices by JAX's collectives and lax.ppermute only.
A program may use at most 128 MiB of HBM per device.

v0:
```python
import jax
import jax.numpy as jnp
from jax import lax
from jax.experimental import pallas as pl
from jax.experimental.pallas import tpu as pltpu
from jax.sharding import PartitionSpec as P

QK = 128
VD = 256
NOPE = 128
ROPE = 64
VDM = 128
KVR = 256
F32 = jnp.float32
BF16 = jnp.bfloat16


def swap(x, axis, distance):
    size = lax.axis_size(axis)
    return lax.ppermute(x, axis, [(i, i ^ distance) for i in range(size)])


def angles_of(positions, half_width):
    inverse = 1.0 / 10000.0 ** (jnp.arange(half_width, dtype=F32) / half_width)
    angles = positions.astype(F32)[:, None] * inverse[None, :]
    return jnp.cos(angles), jnp.sin(angles)


def rotate(vectors, cosine, sine):
    half_width = vectors.shape[-1] // 2
    wide = vectors.astype(F32)
    front, back = wide[..., :half_width], wide[..., half_width:]
    return jnp.concatenate([front * cosine - back * sine, front * sine + back * cosine], axis=-1).astype(BF16)


def dot(a, b, dims=((1,), (0,))):
    return lax.dot_general(a, b, (dims, ((), ())), preferred_element_type=F32)


def gather_keys(own):
    n = lax.axis_size("sp")
    place = lax.axis_index("sp")
    if n != 8 or lax.axis_size("tp") != 2:
        every = lax.all_gather(own, "sp", axis=0, tiled=False)
        return list(every), [jnp.int32(j) for j in range(n)]
    core = lax.axis_index("tp")
    got = []
    for step in (1, 3, 5):
        perm = [(2 * i + t, 2 * (i ^ (step + t)) + t) for i in range(n) for t in range(2)]
        got.append(lax.ppermute(own, ("sp", "tp"), perm))
    last = swap(own, "sp", 7)
    other = swap(jnp.concatenate(got, axis=0), "tp", 1)
    rows = own.shape[0]
    pieces = [own, last] + got + [other[rows * k : rows * (k + 1)] for k in range(3)]
    steps = [jnp.int32(0), jnp.int32(7)] + [s + core for s in (1, 3, 5)] + [s + 1 - core for s in (1, 3, 5)]
    return pieces, [place ^ s for s in steps]


def entering_state(state, log_total):
    n = lax.axis_size("sp")
    place = lax.axis_index("sp")
    heads = state.shape[0]
    total, total_log = state, log_total
    before = jnp.zeros_like(state)
    before_log = jnp.zeros_like(log_total)
    distance = 1
    while distance < n:
        high = lax.reduce_precision(total_log, 8, 7)
        pair = jnp.stack([high, total_log - high], axis=0)
        tail = jnp.broadcast_to(jnp.pad(pair, ((0, 6), (0, 0)))[:, :, None], (8, heads, VD // heads)).reshape(8, VD)
        message = jnp.concatenate([total.astype(BF16).reshape(heads * QK, VD), tail.astype(BF16)], axis=0)
        seen = swap(message, "sp", distance)
        seen_total = seen[: heads * QK].astype(F32).reshape(heads, QK, VD)
        logs = seen[heads * QK : heads * QK + 2].astype(F32)
        seen_log = jnp.sum(logs, axis=0)[:: VD // heads]
        upper = (place & distance) != 0
        before = jnp.where(upper, before + jnp.exp(before_log)[:, None, None] * seen_total, before)
        before_log = jnp.where(upper, before_log + seen_log, before_log)
        if 2 * distance < n:
            early = jnp.where(upper, seen_total, total)
            late = jnp.where(upper, total, seen_total)
            late_log = jnp.where(upper, total_log, seen_log)
            total = jnp.exp(late_log)[:, None, None] * early + late
            total_log = total_log + seen_log
        distance *= 2
    return before


def call(body, outs, args, flops=2_000_000, scratch=()):
    specs = [
        pl.BlockSpec(memory_space=pltpu.SMEM if a.dtype == jnp.int32 else pltpu.VMEM) for a in args
    ]
    shapes = [jax.ShapeDtypeStruct(shape, kind) for shape, kind in outs]
    return pl.pallas_call(
        body,
        out_shape=shapes,
        in_specs=specs,
        out_specs=[pl.BlockSpec(memory_space=pltpu.VMEM) for _ in shapes],
        scratch_shapes=list(scratch),
        cost_estimate=pl.CostEstimate(flops=flops, bytes_accessed=1_000_000, transcendentals=0),
    )(*args)


def turn(wide, cosine, sine):
    half = wide.shape[-1] // 2
    front, back = wide[:, :half], wide[:, half:]
    return jnp.concatenate([front * cosine - back * sine, front * sine + back * cosine], axis=-1)


def pack_body(place, inverse, latent, rope, own, cosine, sine):
    rows = latent.shape[0]
    at = place[0] * rows + lax.broadcasted_iota(jnp.int32, (rows, 128), 0)
    angle = at.astype(F32) * inverse[...]
    cos_all, sin_all = jnp.cos(angle), jnp.sin(angle)
    cosine[...] = cos_all
    sine[...] = sin_all
    half = ROPE // 2
    turned = turn(rope[...].astype(F32), cos_all[:, 64 : 64 + half], sin_all[:, 64 : 64 + half])
    own[:, :KVR] = latent[...]
    own[:, KVR:] = jnp.concatenate([turned, jnp.zeros((rows, 128 - ROPE), F32)], axis=-1).astype(BF16)


def message_of(message, total, logs):
    size = total.shape[0]
    message[:size, :] = total.astype(BF16)
    high = logs.astype(BF16).astype(F32)
    row = lax.broadcasted_iota(jnp.int32, logs.shape, 0)
    message[size:, :] = jnp.where(row == 0, high, logs - high).astype(BF16)


def state_body(query, key, value, decay, cos, sin, rq, rk, col, line, total, total_log, message):
    rows = query.shape[0]
    heads = decay.shape[0]
    first = lax.broadcasted_iota(jnp.int32, (rows, rows), 0)
    second = lax.broadcasted_iota(jnp.int32, (rows, rows), 1)
    lower = (second <= first).astype(F32)
    upper = (first <= second).astype(F32)
    high = lax.Precision.HIGHEST
    padded = jnp.concatenate([decay[...], jnp.zeros((8 - heads, rows), F32)], axis=0)
    sums = lax.dot_general(padded, upper, (((1,), (0,)), ((), ())), precision=high, preferred_element_type=F32)
    down = lax.dot_general(lower, padded, (((1,), (1,)), ((), ())), precision=high, preferred_element_type=F32)
    line[...] = sums
    col[...] = down
    cosine, sine = cos[:, :64], sin[:, :64]
    logs = []
    states = []
    for h in range(heads):
        part = slice(h * QK, (h + 1) * QK)
        rq[:, part] = turn(query[:, part].astype(F32), cosine, sine).astype(BF16)
        turned = turn(key[:, part].astype(F32), cosine, sine).astype(BF16)
        rk[:, part] = turned
        end = down[rows - 1 : rows, h : h + 1]
        faded = (turned.astype(F32) * jnp.exp(end - down[:, h : h + 1])).astype(BF16)
        states.append(dot(faded, value[:, h * VD : (h + 1) * VD], ((0,), (0,))))
        logs.append(jnp.broadcast_to(end, (16, VD // heads)))
    state = jnp.concatenate(states, axis=0)
    log = jnp.concatenate(logs, axis=1)
    total[...] = state
    total_log[...] = log
    message_of(message, state, log)


def fade(logs, heads):
    lanes = VD // heads
    return jnp.concatenate(
        [jnp.broadcast_to(jnp.exp(logs[0:1, h * lanes : h * lanes + 1]), (QK, VD)) for h in range(heads)], axis=0
    )


def opened(seen, heads):
    size = heads * QK
    pieces = seen[size:, :].astype(F32)
    both = pieces[0:1, :] + pieces[1:2, :]
    return seen[:size, :].astype(F32), jnp.broadcast_to(both, (16, VD))


def round_body(upper, seen, total, total_log, before, before_log, message, total_o, log_o, before_o, before_log_o):
    heads = total.shape[0] // QK
    other, other_log = opened(seen, heads)
    up = upper[0].astype(F32)
    before_o[...] = before[...] + up * fade(before_log[...], heads) * other
    before_log_o[...] = before_log[...] + up * other_log
    mine, mine_log = total[...], total_log[...]
    early = up * other + (1.0 - up) * mine
    late = up * mine + (1.0 - up) * other
    late_log = up * mine_log + (1.0 - up) * other_log
    fresh = fade(late_log, heads) * early + late
    fresh_log = mine_log + other_log
    total_o[...] = fresh
    log_o[...] = fresh_log
    message_of(message, fresh, fresh_log)


def query_body(core, rq, rk, value, col, line, query, key_up, cos, sin, intra, q_all):
    rows = rq.shape[0]
    heads = rq.shape[1] // QK
    first = lax.broadcasted_iota(jnp.int32, (rows, rows), 0)
    second = lax.broadcasted_iota(jnp.int32, (rows, rows), 1)
    causal = second <= first
    for h in range(heads):
        part = slice(h * QK, (h + 1) * QK)
        gap = col[:, h : h + 1] - line[h : h + 1, :]
        score = dot(rq[:, part], rk[:, part], ((1,), (1,))) * QK ** (-0.5)
        weight = jnp.where(causal, score * jnp.exp(jnp.where(causal, gap, 0.0)), 0.0).astype(BF16)
        intra[:, h * VD : (h + 1) * VD] = dot(weight, value[:, h * VD : (h + 1) * VD])
    width = NOPE + ROPE
    local = query.shape[1] // width
    half = ROPE // 2
    cosine, sine = cos[:, 64 : 64 + half], sin[:, 64 : 64 + half]
    begin = core[0] * (local * NOPE)
    for h in range(local):
        one = query[:, h * width : (h + 1) * width]
        up = key_up[:, pl.ds(pl.multiple_of(begin + h * NOPE, 128), NOPE)]
        q_all[h * rows : (h + 1) * rows, :KVR] = dot(one[:, :NOPE], up, ((1,), (1,))).astype(BF16)
        turned = turn(one[:, NOPE:].astype(F32), cosine, sine)
        wide = jnp.concatenate([turned, jnp.zeros((rows, 128 - ROPE), F32)], axis=-1)
        q_all[h * rows : (h + 1) * rows, KVR:] = wide.astype(BF16)


def attend_body(seat, q_all, value_up, *rest):
    count = len(rest) - 3
    keys = rest[:count]
    heads_o, logs_o, scores = rest[count:]
    rows = keys[0].shape[0]
    local = q_all.shape[0] // rows
    scale = (NOPE + ROPE) ** (-0.5)
    q = q_all[...]
    at = lax.broadcasted_iota(jnp.int32, (q.shape[0], rows), 0) % rows
    tops = []
    for b in range(count):
        s = dot(q, keys[b][...], ((1,), (1,))) * scale
        if b == 0:
            s = jnp.where(lax.broadcasted_iota(jnp.int32, s.shape, 1) <= at, s, -jnp.inf)
        else:
            s = jnp.where(seat[1 + b] < seat[0], s, -jnp.inf)
        scores[b] = s
        tops.append(s)
    while len(tops) > 1:
        tops = [jnp.maximum(tops[k], tops[k + 1]) if k + 1 < len(tops) else tops[k] for k in range(0, len(tops), 2)]
    top = jnp.max(tops[0], axis=-1, keepdims=True)
    sums = jnp.zeros((q.shape[0], rows), F32)
    weighted = jnp.zeros((q.shape[0], KVR), F32)
    for b in range(count):
        e = jnp.exp(scores[b] - top)
        sums = sums + e
        weighted = weighted + dot(e.astype(BF16), keys[b][:, :KVR])
    total = jnp.sum(sums, axis=-1, keepdims=True)
    log = top + jnp.log(total)
    mean = (weighted / total).astype(BF16)
    begin = seat[1] * (local * VDM)
    for h in range(local):
        part = slice(h * rows, (h + 1) * rows)
        up = value_up[:, pl.ds(pl.multiple_of(begin + h * VDM, 128), VDM)]
        heads_o[:, h * VDM : (h + 1) * VDM] = dot(mean[part], up).astype(BF16)
        logs_o[h : h + 1, :] = jnp.broadcast_to(log[part], (rows, rows)).T[0:1, :]


def heads_body(upper, seen, before, before_log, rq, col, intra, gain, mla_heads, ret_w, mla_w, ret_heads, near):
    heads = rq.shape[1] // QK
    other, _ = opened(seen, heads)
    carried = before[...] + upper[0].astype(F32) * fade(before_log[...], heads) * other
    carried = carried.astype(BF16)
    for h in range(heads):
        part = slice(h * VD, (h + 1) * VD)
        cross = dot(rq[:, h * QK : (h + 1) * QK], carried[h * QK : (h + 1) * QK])
        retained = intra[:, part] + cross * (QK ** (-0.5) * jnp.exp(col[:, h : h + 1]))
        norm = lax.rsqrt(jnp.mean(retained * retained, axis=-1, keepdims=True) + 1e-06)
        ret_heads[:, part] = (retained * norm * gain[:, part]).astype(BF16)
    near[...] = (dot(ret_heads[...], ret_w[...]) + dot(mla_heads[...], mla_w[...])).astype(BF16)


def merge_body(seat, near, ret_heads, mla_heads, ret_w, mla_w, mine, theirs):
    width = near.shape[1]
    half = mine.shape[0]
    far = (dot(ret_heads[...], ret_w[...]) + dot(mla_heads[...], mla_w[...])).astype(BF16)
    upper, lower = far[half:], far[:half]
    here = pl.ds(pl.multiple_of(seat[1] * width, 128), width)
    there = pl.ds(pl.multiple_of((1 - seat[1]) * width, 128), width)
    first = seat[0] == 0
    mine[:, there] = jnp.where(first, lower, upper)
    theirs[:, there] = jnp.where(first, upper, lower)
    mine[:, here] = jnp.where(first, near[:half, :], near[half:, :])
    theirs[:, here] = jnp.where(first, near[half:, :], near[:half, :])


def one(value):
    return jnp.asarray(value, jnp.int32).reshape(1)


def with_kernels(
    ret_query, ret_key, ret_value, log_decay, ret_gain, mla_query,
    kv_latent, rope_key, key_up, value_up, ret_out, mla_out,
):
    rows = ret_query.shape[0]
    heads = ret_value.shape[2] // VD
    local = mla_query.shape[2] // (NOPE + ROPE)
    core, place, side = (lax.axis_index(a) for a in ("tp", "sp", "fs"))
    n = lax.axis_size("sp")
    columns = ret_out.shape[1]
    far_ret = swap(ret_out, "fs", 1)
    far_mla = swap(mla_out, "fs", 1)
    lane = jnp.arange(128)
    power = jnp.where(lane < 64, lane / 64.0, (lane - 64) / 32.0).astype(F32)
    inverse = (1.0 / 10000.0**power)[None]
    own, cos, sin = call(
        pack_body,
        [((rows, 384), BF16), ((rows, 128), F32), ((rows, 128), F32)],
        [one(place), inverse, kv_latent[:, 0], rope_key[:, 0]],
    )
    got = []
    for step in (1, 3, 5):
        perm = [(2 * i + t, 2 * (i ^ (step + t)) + t) for i in range(n) for t in range(2)]
        got.append(lax.ppermute(own, ("sp", "tp"), perm))
    last = swap(own, "sp", 7)
    big = heads * QK
    wide = [((big + 16, VD), BF16), ((big, VD), F32), ((16, VD), F32), ((big, VD), F32), ((16, VD), F32)]
    rq, rk, col, line, total, total_log, message = call(
        state_body,
        [((rows, big), BF16), ((rows, big), BF16), ((rows, 8), F32), ((8, rows), F32), wide[1], wide[2], wide[0]],
        [ret_query[:, 0], ret_key[:, 0], ret_value[:, 0], log_decay[0], cos, sin],
    )
    before, before_log = jnp.zeros((big, VD), F32), jnp.zeros((16, VD), F32)
    distance = 1
    while distance < n:
        seen = swap(message, "sp", distance)
        upper = one((place // distance) % 2)
        if 2 * distance < n:
            message, total, total_log, before, before_log = call(
                round_body, wide, [upper, seen, total, total_log, before, before_log]
            )
        distance *= 2
    intra, q_all = call(
        query_body,
        [((rows, heads * VD), F32), ((local * rows, 384), BF16)],
        [one(core), rq, rk, ret_value[:, 0], col, line, mla_query[:, 0], key_up, cos, sin],
        flops=8_000_000,
    )
    other = [swap(g, "tp", 1) for g in got]
    steps = [0, 7] + [s + core for s in (1, 3, 5)] + [s + 1 - core for s in (1, 3, 5)]
    seat = jnp.stack([jnp.asarray(v, jnp.int32) for v in [place, core] + [place ^ s for s in steps[1:]]])
    keys = [own, last] + got + other
    mla_heads, logs = call(
        attend_body,
        [((rows, local * VDM), BF16), ((local, rows), F32)],
        [seat, q_all, value_up] + keys,
        flops=12_000_000,
        scratch=[pltpu.VMEM((len(keys), local * rows, rows), F32)],
    )
    ret_heads, near = call(
        heads_body,
        [((rows, heads * VD), BF16), ((rows, columns), BF16)],
        [upper, seen, before, before_log, rq, col, intra, ret_gain[None], mla_heads, ret_out, mla_out],
    )
    mine, theirs = call(
        merge_body,
        [((rows // 2, 2 * columns), BF16), ((rows // 2, 2 * columns), BF16)],
        [jnp.stack([core, side]).astype(jnp.int32), near, ret_heads, mla_heads, far_ret, far_mla],
    )
    mixed = (mine.astype(F32) + swap(theirs, "tp", 1).astype(F32)).astype(BF16)
    return mixed[:, None, :], logs[None]


def on_device(
    ret_query, ret_key, ret_value, log_decay, ret_gain, mla_query,
    kv_latent, rope_key, key_up, value_up, ret_out, mla_out,
):
    rows = ret_query.shape[0]
    ret_local = ret_value.shape[2] // VD
    mla_local = mla_query.shape[2] // (NOPE + ROPE)
    core = lax.axis_index("tp")
    place = lax.axis_index("sp")
    fs_size = lax.axis_size("fs")
    positions = place * rows + jnp.arange(rows, dtype=jnp.int32)
    if fs_size == 2:
        far_ret, far_mla = swap(ret_out, "fs", 1), swap(mla_out, "fs", 1)
    else:
        far_ret = lax.all_gather(ret_out, "fs", axis=1, tiled=True)
        far_mla = lax.all_gather(mla_out, "fs", axis=1, tiled=True)

    cos_a, sin_a = angles_of(positions, ROPE // 2)
    own_rope = rotate(rope_key[:, 0], cos_a, sin_a)
    own = jnp.concatenate([kv_latent[:, 0], own_rope, jnp.zeros((rows, 128 - ROPE), BF16)], axis=-1)
    pieces, blocks = gather_keys(own)

    cos_r, sin_r = angles_of(positions, QK // 2)
    cumulative = jnp.cumsum(log_decay[0], axis=-1)
    rq = [rotate(ret_query[:, 0, h * QK : (h + 1) * QK], cos_r, sin_r) for h in range(ret_local)]
    rk = [rotate(ret_key[:, 0, h * QK : (h + 1) * QK], cos_r, sin_r) for h in range(ret_local)]
    rv = [ret_value[:, 0, h * VD : (h + 1) * VD] for h in range(ret_local)]
    tail = jnp.exp(cumulative[:, -1:] - cumulative)
    state = jnp.stack(
        [dot((rk[h].astype(F32) * tail[h][:, None]).astype(BF16), rv[h], ((0,), (0,))) for h in range(ret_local)]
    )
    carried = entering_state(state, cumulative[:, -1])

    scale = QK ** (-0.5)
    causal = jnp.tril(jnp.ones((rows, rows), dtype=bool))
    ret_heads = []
    intra = []
    for h in range(ret_local):
        gap = cumulative[h][:, None] - cumulative[h][None, :]
        score = dot(rq[h], rk[h], ((1,), (1,))) * scale
        weight = jnp.where(causal, score * jnp.exp(jnp.where(causal, gap, 0.0)), 0.0).astype(BF16)
        intra.append(dot(weight, rv[h]))

    head_rows = mla_query[:, 0].reshape(rows, mla_local, NOPE + ROPE)
    up_keys = lax.dynamic_slice_in_dim(key_up, core * (mla_local * NOPE), mla_local * NOPE, 1)
    up_values = lax.dynamic_slice_in_dim(value_up, core * (mla_local * VDM), mla_local * VDM, 1)
    q_parts = []
    for h in range(mla_local):
        absorbed = dot(head_rows[:, h, :NOPE], up_keys[:, h * NOPE : (h + 1) * NOPE], ((1,), (1,))).astype(BF16)
        aq = rotate(head_rows[:, h, NOPE:], cos_a, sin_a)
        q_parts.append(jnp.concatenate([absorbed, aq, jnp.zeros((rows, 128 - ROPE), BF16)], axis=-1))
    q_all = jnp.concatenate(q_parts, axis=0)
    keys = jnp.concatenate(pieces, axis=0)
    key_positions = jnp.concatenate([b * rows + jnp.arange(rows, dtype=jnp.int32) for b in blocks])
    s = dot(q_all, keys, ((1,), (1,))) * ((NOPE + ROPE) ** (-0.5))
    visible = key_positions[None, None, :] <= positions[None, :, None]
    s = jnp.where(visible, s.reshape(mla_local, rows, -1), -jnp.inf).reshape(mla_local * rows, -1)
    top = jnp.max(s, axis=-1, keepdims=True)
    e = jnp.exp(s - top)
    total = jnp.sum(e, axis=-1, keepdims=True)
    weighted = dot(e.astype(BF16), keys[:, :KVR])
    log_weight = (top + jnp.log(total))[:, 0].reshape(1, mla_local, rows)
    mean = (weighted / total).astype(BF16)
    mla_heads = jnp.concatenate(
        [
            dot(mean[h * rows : (h + 1) * rows], up_values[:, h * VDM : (h + 1) * VDM]).astype(BF16)
            for h in range(mla_local)
        ],
        axis=-1,
    )

    for h in range(ret_local):
        cross = dot(rq[h], carried[h].astype(BF16)) * (scale * jnp.exp(cumulative[h])[:, None])
        retained = intra[h] + cross
        norm = lax.rsqrt(jnp.mean(retained * retained, axis=-1, keepdims=True) + 1e-06)
        ret_heads.append((retained * norm * ret_gain[h * VD : (h + 1) * VD]).astype(BF16))
    ret_heads = jnp.concatenate(ret_heads, axis=-1)

    if fs_size == 2:
        near = dot(ret_heads, ret_out) + dot(mla_heads, mla_out)
        far = dot(ret_heads, far_ret) + dot(mla_heads, far_mla)
        first = lax.axis_index("fs") == 0
        partial = jnp.concatenate([jnp.where(first, near, far), jnp.where(first, far, near)], axis=1).astype(BF16)
    else:
        partial = (dot(ret_heads, far_ret) + dot(mla_heads, far_mla)).astype(BF16)
    tp_size = lax.axis_size("tp")
    if tp_size == 2:
        half = rows // 2
        mine = lax.dynamic_slice_in_dim(partial, core * half, half, 0)
        theirs = lax.dynamic_slice_in_dim(partial, (1 - core) * half, half, 0)
        mixed = (mine.astype(F32) + swap(theirs, "tp", 1).astype(F32)).astype(BF16)
    else:
        mixed = lax.psum_scatter(partial, "tp", scatter_dimension=0, tiled=True)
    return mixed[:, None, :], log_weight


def solution(mesh):
    in_specs = (
        P("sp", "fs", "tp"),
        P("sp", "fs", "tp"),
        P("sp", "fs", "tp"),
        P("fs", "tp", "sp"),
        P("tp"),
        P("sp", "fs", "tp"),
        P("sp", "fs", None),
        P("sp", "fs", None),
        P(),
        P(),
        P("tp", "fs"),
        P("tp", "fs"),
    )
    out_specs = (P(("sp", "tp"), "fs", None), P("fs", "tp", "sp"))
    small = mesh.shape["sp"] == 8 and mesh.shape["fs"] == 2 and mesh.shape["tp"] == 2
    body = with_kernels if small else on_device
    return jax.shard_map(body, mesh=mesh, in_specs=in_specs, out_specs=out_specs, check_vma=False)
```

profile of v0, /device:TPU:0, one launch (start us, length us, event | category | flops | bytes accessed | tf_op | source)
XLA Modules:
  0.0 59.0 jit_solution(6388614440297108340)
XLA Ops:
  0.6 3.0 %collective-permute-start.10 = (bf16[512,1024]{1,0:T(8,128)(2,1)}, bf16[512,1024]{1,0:T(8,128)(2,1)S(1)}, u32[]{:S(2)}, u32[]{:S(2)}) collective-permute-start(bf16[512,1024]{1,0:T(8,128)(2,1)} %ret_w.1), channel_id=1, source_target_pairs={{0,2},{2,0},{1,3},{3,1},{4,6},{6,4},{5,7},{7,5},{8,10},{10,8},{9,1... | collective-permute-start | bytes 3145736 | tf_op jit(solution)/shard_map/ppermute | solution.py:20
  3.7 1.4 %copy.14 = bf16[128,1,64]{2,0,1:T(8,128)(2,1)} copy(bf16[128,1,64]{0,2,1:T(8,128)(2,1)} %param.19) | data formatting | bytes 32768 | tf_op args[7]
  5.2 0.5 fusion.5.inverse
  5.7 1.9 %shard_map.131 = (bf16[128,384]{1,0:T(8,128)(2,1)}, f32[128,128]{1,0:T(8,128)}, f32[128,128]{1,0:T(8,128)}) custom-call(s32[1]{0:T(128)} %bitcast.9.place, f32[1,128]{1,0:T(1,128)} %fusion.5.inverse, bf16[128,256]{1,0:T(8,128)(2,1)} %bitcast.28, bf16[128,64]{1,0:T(8,128)(2,1)} %bitcast.27), custom_call_target="tpu_custom_call" | custom-call | flops 2000000 | bytes 1000000 | tf_op jit(solution)/shard_map/pallas_call | solution.py:94
  7.6 2.3 %shard_map.132 = (bf16[128,256]{1,0:T(8,128)(2,1)}, bf16[128,256]{1,0:T(8,128)(2,1)}, f32[128,8]{1,0:T(8,128)}, f32[8,128]{1,0:T(8,128)}, f32[256,256]{1,0:T(8,1...) custom-call(bf16[128,256]{1,0:T(8,128)(2,1)} %bitcast.29, bf16[128,256]{1,0:T(8,128)(2,1)} %bitcast.30, ...), custom_call_target="tpu_custom_call" | custom-call | flops 2000000 | bytes 1000000 | tf_op jit(solution)/shard_map/pallas_call | solution.py:94
  9.9 2.0 %collective-permute-start = (bf16[272,256]{1,0:T(8,128)(2,1)}, bf16[272,256]{1,0:T(8,128)(2,1)S(1)}, u32[]{:S(2)}, u32[]{:S(2)}) collective-permute-start(bf16[272,256]{1,0:T(8,128)(2,1)} %get-tuple-element.30), channel_id=1, source_target_pairs={{0,4},{4,0},{8,12},{12,8},{16,20},{20,16},{24,28},{28,24},{1,5},{5... | collective-permute-start | bytes 417800 | tf_op jit(solution)/shard_map/ppermute | solution.py:20
  11.9 3.4 %collective-permute-done.seen = bf16[272,256]{1,0:T(8,128)(2,1)S(1)} collective-permute-done((bf16[272,256]{1,0:T(8,128)(2,1)}, bf16[272,256]{1,0:T(8,128)(2,1)S(1)}, u32[]{:S(2)}, u32[]{:S(2)}) %collective-permute-start) | collective-permute-done | bytes 139296 | tf_op jit(solution)/shard_map/ppermute | solution.py:20
  15.3 0.6 %broadcast_in_dim.17.before_log = f32[16,256]{1,0:T(8,128)} broadcast(f32[]{:T(128)} %constant.82.clone.1), dimensions={} | broadcast | bytes 16388 | tf_op jit(solution)/shard_map/broadcast_in_dim | solution.py:322
  15.9 0.7 %broadcast_in_dim.16.before = f32[256,256]{1,0:T(8,128)} broadcast(f32[]{:T(128)} %constant.82.clone.1), dimensions={} | broadcast | bytes 262148 | tf_op jit(solution)/shard_map/broadcast_in_dim | solution.py:322
  16.6 2.1 %shard_map.133 = (bf16[272,256]{1,0:T(8,128)(2,1)}, f32[256,256]{1,0:T(8,128)}, f32[16,256]{1,0:T(8,128)}, f32[256,256]{1,0:T(8,128)}, f32[16,256]{1,0:T(8,128)}) custom-call(s32[1]{0:T(128)} %bitcast.4.upper, bf16[272,256]{1,0:T(8,128)(2,1)} %copy-done.4, f32[256,256]{1,0:T(8,128)} %get-tuple-element.31.total, f32[16,256]{1,0:T(8,128)} %get-tuple-element.32.total_log, ...), custom_call_target="tpu_custom_call" | custom-call | flops 2000000 | bytes 1000000 | tf_op jit(solution)/shard_map/pallas_call | solution.py:94
  18.7 2.0 %collective-permute-start.1 = (bf16[272,256]{1,0:T(8,128)(2,1)}, bf16[272,256]{1,0:T(8,128)(2,1)S(1)}, u32[]{:S(2)}, u32[]{:S(2)}) collective-permute-start(bf16[272,256]{1,0:T(8,128)(2,1)} %get-tuple-element.33), channel_id=1, source_target_pairs={{0,8},{4,12},{8,0},{12,4},{16,24},{20,28},{24,16},{28,20},{1,9},{5... | collective-permute-start | bytes 417800 | tf_op jit(solution)/shard_map/ppermute | solution.py:20
  20.7 3.5 %collective-permute-start.6 = (bf16[128,384]{1,0:T(8,128)(2,1)S(1)}, bf16[128,384]{1,0:T(8,128)(2,1)S(1)}, u32[]{:S(2)}, u32[]{:S(2)}) collective-permute-start(bf16[128,384]{1,0:T(8,128)(2,1)S(1)} %copy-done.5), channel_id=1, source_target_pairs={{0,20},{1,25},{4,16},{5,29},{8,28},{9,17},{12,24},{13,21},{16,4},{... | collective-permute-start | bytes 294920 | tf_op jit(solution)/shard_map/ppermute | solution.py:313
  24.2 0.4 collective-permute-start.5
  24.6 5.6 %collective-permute-done.6.rest_4_ = bf16[128,384]{1,0:T(8,128)(2,1)S(1)} collective-permute-done((bf16[128,384]{1,0:T(8,128)(2,1)S(1)}, bf16[128,384]{1,0:T(8,128)(2,1)S(1)}, u32[]{:S(2)}, u32[]{:S(2)}) %collective-permute-start.6) | collective-permute-done | bytes 98336 | tf_op jit(solution)/shard_map/ppermute | solution.py:313
  30.2 0.5 collective-permute-start.4
  30.7 0.5 collective-permute-done.5.rest_3_
  31.2 2.5 %collective-permute-start.3 = (bf16[128,384]{1,0:T(8,128)(2,1)S(1)}, bf16[128,384]{1,0:T(8,128)(2,1)S(1)}, u32[]{:S(2)}, u32[]{:S(2)}) collective-permute-start(bf16[128,384]{1,0:T(8,128)(2,1)S(1)} %copy-done.5), channel_id=1, source_target_pairs={{0,28},{4,24},{8,20},{12,16},{16,12},{20,8},{24,4},{28,0},{1,29},{... | collective-permute-start | bytes 294920 | tf_op jit(solution)/shard_map/ppermute | solution.py:20
  33.7 0.6 %copy-done.3 = bf16[272,256]{1,0:T(8,128)(2,1)} copy-done((bf16[272,256]{1,0:T(8,128)(2,1)}, bf16[272,256]{1,0:T(8,128)(2,1)S(1)}, u32[]{:S(2)}) %copy-start.3) | copy-done | bytes 139288
  34.3 2.0 %shard_map.134 = (bf16[272,256]{1,0:T(8,128)(2,1)}, f32[256,256]{1,0:T(8,128)}, f32[16,256]{1,0:T(8,128)}, f32[256,256]{1,0:T(8,128)}, f32[16,256]{1,0:T(8,128)}) custom-call(s32[1]{0:T(128)} %bitcast.3.upper, bf16[272,256]{1,0:T(8,128)(2,1)} %copy-done.3, f32[256,256]{1,0:T(8,128)} %get-tuple-element.34.total, f32[16,256]{1,0:T(8,128)} %get-tuple-element.35.total_log, ...), custom_call_target="tpu_custom_call" | custom-call | flops 2000000 | bytes 1000000 | tf_op jit(solution)/shard_map/pallas_call | solution.py:94
  36.5 0.7 %stack.45.seat = s32[9]{0:T(128)} concatenate(s32[1]{0:T(128)} %bitcast.9.place, s32[1]{0:T(128)} %bitcast.core, s32[1]{0:T(128)} %bitcast.14, s32[1]{0:T(128)} %bitcast.15, s32[1]{0:T(128)} %bitcast.16, s32[1]{0:T(128)} %bitcast.17, s32[1]{0:T(128)} %bitcast.18, s32[1]{0:T(128)} %bitcast.19, s32[1]{0:T(128)} %bitcast.20), dimensions={0} | concatenate | bytes 72 | tf_op jit(solution)/shard_map/stack | solution.py:340
  37.1 2.9 %shard_map.135 = (f32[128,512]{1,0:T(8,128)}, bf16[512,384]{1,0:T(8,128)(2,1)}) custom-call(s32[1]{0:T(128)} %bitcast.core, bf16[128,256]{1,0:T(8,128)(2,1)} %get-tuple-element.41.rq, bf16[128,256]{1,0:T(8,128)(2,1)} %get-tuple-element.43.rk, bf16[128,512]{1,0:T(8,128)(2,1)} %bitcast.25, f32[128,8]{1,0:T(8,128)} %get-tuple-element.42.col, ...), custom_call_target="tpu_custom_call" | custom-call | flops 8000000 | bytes 1000000 | tf_op jit(solution)/shard_map/pallas_call | solution.py:94
  40.1 0.5 collective-permute-start.7
  40.7 0.7 %pad_add_fusion.seat = s32[2]{0:T(128)} fusion(s32[1]{0:T(128)} %bitcast.1, s32[1]{0:T(128)} %bitcast.core), kind=kLoop, calls=%fused_computation.10 | loop fusion | flops 2 | bytes 16 | tf_op jit(solution)/shard_map/stack | solution.py:357
  41.6 0.4 copy-done.11
  42.2 5.0 %shard_map.136 = (bf16[128,512]{1,0:T(8,128)(2,1)}, f32[4,128]{1,0:T(4,128)}) custom-call(s32[9]{0:T(128)} %stack.45.seat, bf16[512,384]{1,0:T(8,128)(2,1)} %get-tuple-element.46.q_all, bf16[256,1024]{1,0:T(8,128)(2,1)} %value_up.1, bf16[128,384]{1,0:T(8,128)(2,1)} %get-tuple-element.47.rest_0_, bf16[128,384]{1,0:T(8,128)(2,1)} %copy-done.9, ...), custom_call_target="tpu_custom_call" | custom-call | flops 12000000 | bytes 1000000 | tf_op jit(solution)/shard_map/pallas_call | solution.py:94
  47.3 0.6 %copy-done.2 = bf16[272,256]{1,0:T(8,128)(2,1)} copy-done((bf16[272,256]{1,0:T(8,128)(2,1)}, bf16[272,256]{1,0:T(8,128)(2,1)S(1)}, u32[]{:S(2)}) %copy-start.2) | copy-done | bytes 139288
  47.9 3.2 %shard_map.137 = (bf16[128,512]{1,0:T(8,128)(2,1)}, bf16[128,1024]{1,0:T(8,128)(2,1)}) custom-call(s32[1]{0:T(128)} %bitcast.2.upper, bf16[272,256]{1,0:T(8,128)(2,1)} %copy-done.2, f32[256,256]{1,0:T(8,128)} %get-tuple-element.39.before, f32[16,256]{1,0:T(8,128)} %get-tuple-element.40.before_log, bf16[128,256]{1,0:T(8,128)(2,1)} %get-tuple-element.41.rq, ...), custom_call_target="tpu_custom_call" | custom-call | flops 2000000 | bytes 1000000 | tf_op jit(solution)/shard_map/pallas_call | solution.py:94
  51.1 0.9 %copy-done = bf16[512,1024]{1,0:T(8,128)(2,1)} copy-done((bf16[512,1024]{1,0:T(8,128)(2,1)}, bf16[512,1024]{1,0:T(8,128)(2,1)S(1)}, u32[]{:S(2)}) %copy-start) | copy-done | bytes 1048600
  52.1 0.4 copy-done.1
  52.5 3.0 %shard_map.138 = (bf16[64,2048]{1,0:T(8,128)(2,1)}, bf16[64,2048]{1,0:T(8,128)(2,1)}) custom-call(s32[2]{0:T(128)} %pad_add_fusion.seat, bf16[128,1024]{1,0:T(8,128)(2,1)} %get-tuple-element.49.near, bf16[128,512]{1,0:T(8,128)(2,1)} %get-tuple-element.50.ret_heads, bf16[128,512]{1,0:T(8,128)(2,1)} %get-tuple-element.48.mla_heads, bf16[512,1024]{1,0:T(8,128)(2,1)} %copy-done, ...), custom_call_target="tpu_custom_call" | custom-call | flops 2000000 | bytes 1000000 | tf_op jit(solution)/shard_map/pallas_call | solution.py:94
  55.9 1.4 %collective-permute-done.12 = bf16[64,2048]{1,0:T(8,128)(2,1)S(1)} collective-permute-done((bf16[64,2048]{1,0:T(8,128)(2,1)}, bf16[64,2048]{1,0:T(8,128)(2,1)S(1)}, u32[]{:S(2)}, u32[]{:S(2)}) %collective-permute-start.12) | collective-permute-done | bytes 262176 | tf_op jit(solution)/shard_map/ppermute | solution.py:20
  57.3 1.7 %fusion = bf16[64,1,2048]{2,0,1:T(8,128)(2,1)} fusion(bf16[64,2048]{1,0:T(8,128)(2,1)S(1)} %collective-permute-done.12, bf16[64,2048]{1,0:T(8,128)(2,1)} %get-tuple-element.51), kind=kLoop, calls=%fused_computation.1 | loop fusion | flops 524288 | bytes 786432 | tf_op jit(solution)/shard_map/broadcast_in_dim | solution.py:360
  (35 shorter events, 1.1 us)
Async XLA Ops:
  0.6 50.5 %collective-permute-start.10 = (bf16[512,1024]{1,0:T(8,128)(2,1)}, bf16[512,1024]{1,0:T(8,128)(2,1)S(1)}, u32[]{:S(2)}, u32[]{:S(2)}) collective-permute-start(bf16[512,1024]{1,0:T(8,128)(2,1)} %ret_w.1), channel_id=1, source_target_pairs={{0,2},{2,0},{1,3},{3,1},{4,6},{6,4},{5,7},{7,5},{8,10},{10,8},{9,1... | collective-permute-start | bytes 3145736 | tf_op jit(solution)/shard_map/ppermute | solution.py:20
  3.7 47.5 %collective-permute-start.11 = (bf16[512,1024]{1,0:T(8,128)(2,1)}, bf16[512,1024]{1,0:T(8,128)(2,1)S(1)}, u32[]{:S(2)}, u32[]{:S(2)}) collective-permute-start(bf16[512,1024]{1,0:T(8,128)(2,1)} %mla_w.1), channel_id=1, source_target_pairs={{0,2},{2,0},{1,3},{3,1},{4,6},{6,4},{5,7},{7,5},{8,10},{10,8},{9,1... | collective-permute-start | bytes 3145736 | tf_op jit(solution)/shard_map/ppermute | solution.py:20
  9.9 5.3 %collective-permute-start = (bf16[272,256]{1,0:T(8,128)(2,1)}, bf16[272,256]{1,0:T(8,128)(2,1)S(1)}, u32[]{:S(2)}, u32[]{:S(2)}) collective-permute-start(bf16[272,256]{1,0:T(8,128)(2,1)} %get-tuple-element.30), channel_id=1, source_target_pairs={{0,4},{4,0},{8,12},{12,8},{16,20},{20,16},{24,28},{28,24},{1,5},{5... | collective-permute-start | bytes 417800 | tf_op jit(solution)/shard_map/ppermute | solution.py:20
  15.3 1.4 %copy-start.4 = (bf16[272,256]{1,0:T(8,128)(2,1)}, bf16[272,256]{1,0:T(8,128)(2,1)S(1)}, u32[]{:S(2)}) copy-start(bf16[272,256]{1,0:T(8,128)(2,1)S(1)} %collective-permute-done.seen) | copy-start | bytes 417796
  16.6 4.1 %copy-start.5 = (bf16[128,384]{1,0:T(8,128)(2,1)S(1)}, bf16[128,384]{1,0:T(8,128)(2,1)}, u32[]{:S(2)}) copy-start(bf16[128,384]{1,0:T(8,128)(2,1)} %get-tuple-element.47.rest_0_) | copy-start | bytes 294916
  18.7 14.9 %collective-permute-start.1 = (bf16[272,256]{1,0:T(8,128)(2,1)}, bf16[272,256]{1,0:T(8,128)(2,1)S(1)}, u32[]{:S(2)}, u32[]{:S(2)}) collective-permute-start(bf16[272,256]{1,0:T(8,128)(2,1)} %get-tuple-element.33), channel_id=1, source_target_pairs={{0,8},{4,12},{8,0},{12,4},{16,24},{20,28},{24,16},{28,20},{1,9},{5... | collective-permute-start | bytes 417800 | tf_op jit(solution)/shard_map/ppermute | solution.py:20
  20.7 9.5 %collective-permute-start.6 = (bf16[128,384]{1,0:T(8,128)(2,1)S(1)}, bf16[128,384]{1,0:T(8,128)(2,1)S(1)}, u32[]{:S(2)}, u32[]{:S(2)}) collective-permute-start(bf16[128,384]{1,0:T(8,128)(2,1)S(1)} %copy-done.5), channel_id=1, source_target_pairs={{0,20},{1,25},{4,16},{5,29},{8,28},{9,17},{12,24},{13,21},{16,4},{... | collective-permute-start | bytes 294920 | tf_op jit(solution)/shard_map/ppermute | solution.py:313
  24.2 6.9 %collective-permute-start.5 = (bf16[128,384]{1,0:T(8,128)(2,1)S(1)}, bf16[128,384]{1,0:T(8,128)(2,1)S(1)}, u32[]{:S(2)}, u32[]{:S(2)}) collective-permute-start(bf16[128,384]{1,0:T(8,128)(2,1)S(1)} %copy-done.5), channel_id=1, source_target_pairs={{0,12},{1,17},{4,8},{5,21},{8,4},{9,25},{12,0},{13,29},{16,28},{17... | collective-permute-start | bytes 294920 | tf_op jit(solution)/shard_map/ppermute | solution.py:313
  30.2 6.1 %copy-start.6 = (bf16[128,384]{1,0:T(8,128)(2,1)}, bf16[128,384]{1,0:T(8,128)(2,1)S(1)}, u32[]{:S(2)}) copy-start(bf16[128,384]{1,0:T(8,128)(2,1)S(1)} %collective-permute-done.6.rest_4_) | copy-start | bytes 294916
  30.2 6.1 %collective-permute-start.4 = (bf16[128,384]{1,0:T(8,128)(2,1)S(1)}, bf16[128,384]{1,0:T(8,128)(2,1)S(1)}, u32[]{:S(2)}, u32[]{:S(2)}) collective-permute-start(bf16[128,384]{1,0:T(8,128)(2,1)S(1)} %copy-done.5), channel_id=1, source_target_pairs={{0,4},{1,9},{4,0},{5,13},{8,12},{9,1},{12,8},{13,5},{16,20},{17,25... | collective-permute-start | bytes 294920 | tf_op jit(solution)/shard_map/ppermute | solution.py:313
  31.2 8.8 %copy-start.7 = (bf16[128,384]{1,0:T(8,128)(2,1)}, bf16[128,384]{1,0:T(8,128)(2,1)S(1)}, u32[]{:S(2)}) copy-start(bf16[128,384]{1,0:T(8,128)(2,1)S(1)} %collective-permute-done.5.rest_3_) | copy-start | bytes 294916
  31.2 8.8 %collective-permute-start.3 = (bf16[128,384]{1,0:T(8,128)(2,1)S(1)}, bf16[128,384]{1,0:T(8,128)(2,1)S(1)}, u32[]{:S(2)}, u32[]{:S(2)}) collective-permute-start(bf16[128,384]{1,0:T(8,128)(2,1)S(1)} %copy-done.5), channel_id=1, source_target_pairs={{0,28},{4,24},{8,20},{12,16},{16,12},{20,8},{24,4},{28,0},{1,29},{... | collective-permute-start | bytes 294920 | tf_op jit(solution)/shard_map/ppermute | solution.py:20
  33.6 0.7 %copy-start.3 = (bf16[272,256]{1,0:T(8,128)(2,1)}, bf16[272,256]{1,0:T(8,128)(2,1)S(1)}, u32[]{:S(2)}) copy-start(bf16[272,256]{1,0:T(8,128)(2,1)S(1)} %collective-permute-done.1.seen) | copy-start | bytes 417796
  33.6 6.5 %collective-permute-start.9 = (bf16[128,384]{1,0:T(8,128)(2,1)S(1)}, bf16[128,384]{1,0:T(8,128)(2,1)S(1)}, u32[]{:S(2)}, u32[]{:S(2)}) collective-permute-start(bf16[128,384]{1,0:T(8,128)(2,1)S(1)} %collective-permute-done.6.rest_4_), channel_id=1, source_target_pairs={{0,1},{1,0},{2,3},{3,2},{4,5},{5,4},{6,7},{7,6},{8,9},{9,8},{10,11... | collective-permute-start | bytes 294920 | tf_op jit(solution)/shard_map/ppermute | solution.py:20
  36.3 3.8 %copy-start.8 = (bf16[128,384]{1,0:T(8,128)(2,1)}, bf16[128,384]{1,0:T(8,128)(2,1)S(1)}, u32[]{:S(2)}) copy-start(bf16[128,384]{1,0:T(8,128)(2,1)S(1)} %collective-permute-done.4.rest_2_) | copy-start | bytes 294916
  36.3 10.9 %collective-permute-start.2 = (bf16[272,256]{1,0:T(8,128)(2,1)}, bf16[272,256]{1,0:T(8,128)(2,1)S(1)}, u32[]{:S(2)}, u32[]{:S(2)}) collective-permute-start(bf16[272,256]{1,0:T(8,128)(2,1)} %get-tuple-element.38), channel_id=1, source_target_pairs={{0,16},{4,20},{8,24},{12,28},{16,0},{20,4},{24,8},{28,12},{1,17},{... | collective-permute-start | bytes 417800 | tf_op jit(solution)/shard_map/ppermute | solution.py:20
  40.0 1.6 %copy-start.9 = (bf16[128,384]{1,0:T(8,128)(2,1)}, bf16[128,384]{1,0:T(8,128)(2,1)S(1)}, u32[]{:S(2)}) copy-start(bf16[128,384]{1,0:T(8,128)(2,1)S(1)} %collective-permute-done.3.rest_1_) | copy-start | bytes 294916
  40.0 1.4 %collective-permute-start.8 = (bf16[128,384]{1,0:T(8,128)(2,1)S(1)}, bf16[128,384]{1,0:T(8,128)(2,1)S(1)}, u32[]{:S(2)}, u32[]{:S(2)}) collective-permute-start(bf16[128,384]{1,0:T(8,128)(2,1)S(1)} %collective-permute-done.5.rest_3_), channel_id=1, source_target_pairs={{0,1},{1,0},{2,3},{3,2},{4,5},{5,4},{6,7},{7,6},{8,9},{9,8},{10,11... | collective-permute-start | bytes 294920 | tf_op jit(solution)/shard_map/ppermute | solution.py:20
  40.1 1.5 %copy-start.10 = (bf16[128,384]{1,0:T(8,128)(2,1)}, bf16[128,384]{1,0:T(8,128)(2,1)S(1)}, u32[]{:S(2)}) copy-start(bf16[128,384]{1,0:T(8,128)(2,1)S(1)} %collective-permute-done.9.rest_7_) | copy-start | bytes 294916
  40.1 1.5 %collective-permute-start.7 = (bf16[128,384]{1,0:T(8,128)(2,1)S(1)}, bf16[128,384]{1,0:T(8,128)(2,1)S(1)}, u32[]{:S(2)}, u32[]{:S(2)}) collective-permute-start(bf16[128,384]{1,0:T(8,128)(2,1)S(1)} %collective-permute-done.4.rest_2_), channel_id=1, source_target_pairs={{0,1},{1,0},{2,3},{3,2},{4,5},{5,4},{6,7},{7,6},{8,9},{9,8},{10,11... | collective-permute-start | bytes 294920 | tf_op jit(solution)/shard_map/ppermute | solution.py:20
  41.4 0.6 %copy-start.11 = (bf16[128,384]{1,0:T(8,128)(2,1)}, bf16[128,384]{1,0:T(8,128)(2,1)S(1)}, u32[]{:S(2)}) copy-start(bf16[128,384]{1,0:T(8,128)(2,1)S(1)} %collective-permute-done.8.rest_6_) | copy-start | bytes 294916
  41.6 0.6 %copy-start.12 = (bf16[128,384]{1,0:T(8,128)(2,1)}, bf16[128,384]{1,0:T(8,128)(2,1)S(1)}, u32[]{:S(2)}) copy-start(bf16[128,384]{1,0:T(8,128)(2,1)S(1)} %collective-permute-done.7.rest_5_) | copy-start | bytes 294916
  47.2 0.7 %copy-start.2 = (bf16[272,256]{1,0:T(8,128)(2,1)}, bf16[272,256]{1,0:T(8,128)(2,1)S(1)}, u32[]{:S(2)}) copy-start(bf16[272,256]{1,0:T(8,128)(2,1)S(1)} %collective-permute-done.2.seen) | copy-start | bytes 417796
  51.1 1.0 %copy-start = (bf16[512,1024]{1,0:T(8,128)(2,1)}, bf16[512,1024]{1,0:T(8,128)(2,1)S(1)}, u32[]{:S(2)}) copy-start(bf16[512,1024]{1,0:T(8,128)(2,1)S(1)} %collective-permute-done.10.ret_w) | copy-start | bytes 3145732
  51.1 1.3 %copy-start.1 = (bf16[512,1024]{1,0:T(8,128)(2,1)}, bf16[512,1024]{1,0:T(8,128)(2,1)S(1)}, u32[]{:S(2)}) copy-start(bf16[512,1024]{1,0:T(8,128)(2,1)S(1)} %collective-permute-done.11.mla_w) | copy-start | bytes 3145732
  55.5 1.7 %collective-permute-start.12 = (bf16[64,2048]{1,0:T(8,128)(2,1)}, bf16[64,2048]{1,0:T(8,128)(2,1)S(1)}, u32[]{:S(2)}, u32[]{:S(2)}) collective-permute-start(bf16[64,2048]{1,0:T(8,128)(2,1)} %get-tuple-element.52), channel_id=1, source_target_pairs={{0,1},{1,0},{2,3},{3,2},{4,5},{5,4},{6,7},{7,6},{8,9},{9,8},{10,11... | collective-permute-start | bytes 786440 | tf_op jit(solution)/shard_map/ppermute | solution.py:20
where the time goes:
time: 59.4 us; the launch traced here: 59 us
  Pallas kernels  22.5 us (38%)
  starting transfers between devices  15 us (25%)
  waiting for transfers between devices  11.1 us (19%)
  local copies, waits for them, and re-layouts  6.7 us (11%)
  other arithmetic  2.91 us (5%)
  between operations  0.82 us (1%)
    pallas_call x8, Pallas kernels, call(): pl.pallas_call(body, out_shape=shapes, in_specs=specs, out_specs=[pl.Bloc...  22.5 us
    ppermute x10, starting transfers between devices, swap(): return lax.ppermute(x, axis, [(i, i ^ distance) for i in range(size)])  10.5 us
    ppermute x3, waiting for transfers between devices, with_kernels(): got.append(lax.ppermute(own, ('sp', 'tp'), perm))  6.05 us
    ppermute x10, waiting for transfers between devices, swap(): return lax.ppermute(x, axis, [(i, i ^ distance) for i in range(size)])  5.05 us
    unnamed x27, local copies, waits for them, and re-layouts  4.69 us
    ppermute x3, starting transfers between devices, with_kernels(): got.append(lax.ppermute(own, ('sp', 'tp'), perm))  4.44 us
    broadcast_in_dim x1, other arithmetic, with_kernels(): return (mixed[:, None, :], logs[None])  1.72 us
    broadcast_in_dim x2, local copies, waits for them, and re-layouts, with_kernels(): before, before_log = (jnp.zeros((big, VD), F32), jnp.zeros((16, VD), F32))  1.34 us
  transfers between devices with their start and end apart: 13, of which 6 were waited for; matrix products, arithmetic and copies ran while one was open for 8% of the time, Pallas kernels for 33%

commit v1 on v0

--- a/solution.py
+++ b/solution.py
@@ -90,13 +90,15 @@
     specs = [
         pl.BlockSpec(memory_space=pltpu.SMEM if a.dtype == jnp.int32 else pltpu.VMEM) for a in args
     ]
-    shapes = [jax.ShapeDtypeStruct(shape, kind) for shape, kind in outs]
+    shapes = [pltpu.VMEM(shape, kind) for shape, kind in outs]
+    args = [a if a.dtype == jnp.int32 else pltpu.with_memory_space_constraint(a, pltpu.VMEM) for a in args]
     return pl.pallas_call(
         body,
         out_shape=shapes,
         in_specs=specs,
         out_specs=[pl.BlockSpec(memory_space=pltpu.VMEM) for _ in shapes],
         scratch_shapes=list(scratch),
+        compiler_params=pltpu.CompilerParams(vmem_limit_bytes=16 * 1024 * 1024),
         cost_estimate=pl.CostEstimate(flops=flops, bytes_accessed=1_000_000, transcendentals=0),
     )(*args)
 
@@ -178,8 +180,12 @@
     heads = total.shape[0] // QK
     other, other_log = opened(seen, heads)
     up = upper[0].astype(F32)
-    before_o[...] = before[...] + up * fade(before_log[...], heads) * other
-    before_log_o[...] = before_log[...] + up * other_log
+    if before is None:
+        before_o[...] = up * other
+        before_log_o[...] = up * other_log
+    else:
+        before_o[...] = before[...] + up * fade(before_log[...], heads) * other
+        before_log_o[...] = before_log[...] + up * other_log
     mine, mine_log = total[...], total_log[...]
     early = up * other + (1.0 - up) * mine
     late = up * mine + (1.0 - up) * other
@@ -189,6 +195,10 @@
     total_o[...] = fresh
     log_o[...] = fresh_log
     message_of(message, fresh, fresh_log)
+
+
+def first_body(upper, seen, total, total_log, message, total_o, log_o, before_o, before_log_o):
+    round_body(upper, seen, total, total_log, None, None, message, total_o, log_o, before_o, before_log_o)
 
 
 def query_body(core, rq, rk, value, col, line, query, key_up, cos, sin, intra, q_all):
@@ -217,7 +227,7 @@
         q_all[h * rows : (h + 1) * rows, KVR:] = wide.astype(BF16)
 
 
-def attend_body(seat, q_all, value_up, *rest):
+def attend_body(place, core, q_all, value_up, *rest):
     count = len(rest) - 3
     keys = rest[:count]
     heads_o, logs_o, scores = rest[count:]
@@ -227,12 +237,14 @@
     q = q_all[...]
     at = lax.broadcasted_iota(jnp.int32, (q.shape[0], rows), 0) % rows
     tops = []
+    t = core[0]
+    steps = [0, 7] + [d + t for d in (1, 3, 5)] + [d + 1 - t for d in (1, 3, 5)]
     for b in range(count):
         s = dot(q, keys[b][...], ((1,), (1,))) * scale
         if b == 0:
             s = jnp.where(lax.broadcasted_iota(jnp.int32, s.shape, 1) <= at, s, -jnp.inf)
         else:
-            s = jnp.where(seat[1 + b] < seat[0], s, -jnp.inf)
+            s = jnp.where((place[0] ^ steps[b]) < place[0], s, -jnp.inf)
         scores[b] = s
         tops.append(s)
     while len(tops) > 1:
@@ -247,7 +259,7 @@
     total = jnp.sum(sums, axis=-1, keepdims=True)
     log = top + jnp.log(total)
     mean = (weighted / total).astype(BF16)
-    begin = seat[1] * (local * VDM)
+    begin = core[0] * (local * VDM)
     for h in range(local):
         part = slice(h * rows, (h + 1) * rows)
         up = value_up[:, pl.ds(pl.multiple_of(begin + h * VDM, 128), VDM)]
@@ -269,14 +281,14 @@
     near[...] = (dot(ret_heads[...], ret_w[...]) + dot(mla_heads[...], mla_w[...])).astype(BF16)
 
 
-def merge_body(seat, near, ret_heads, mla_heads, ret_w, mla_w, mine, theirs):
+def merge_body(core, side, near, ret_heads, mla_heads, ret_w, mla_w, mine, theirs):
     width = near.shape[1]
     half = mine.shape[0]
     far = (dot(ret_heads[...], ret_w[...]) + dot(mla_heads[...], mla_w[...])).astype(BF16)
     upper, lower = far[half:], far[:half]
-    here = pl.ds(pl.multiple_of(seat[1] * width, 128), width)
-    there = pl.ds(pl.multiple_of((1 - seat[1]) * width, 128), width)
-    first = seat[0] == 0
+    here = pl.ds(pl.multiple_of(side[0] * width, 128), width)
+    there = pl.ds(pl.multiple_of((1 - side[0]) * width, 128), width)
+    first = core[0] == 0
     mine[:, there] = jnp.where(first, lower, upper)
     theirs[:, there] = jnp.where(first, upper, lower)
     mine[:, here] = jnp.where(first, near[:half, :], near[half:, :])
@@ -319,15 +331,14 @@
         [((rows, big), BF16), ((rows, big), BF16), ((rows, 8), F32), ((8, rows), F32), wide[1], wide[2], wide[0]],
         [ret_query[:, 0], ret_key[:, 0], ret_value[:, 0], log_decay[0], cos, sin],
     )
-    before, before_log = jnp.zeros((big, VD), F32), jnp.zeros((16, VD), F32)
+    carry = []
     distance = 1
     while distance < n:
         seen = swap(message, "sp", distance)
         upper = one((place // distance) % 2)
         if 2 * distance < n:
-            message, total, total_log, before, before_log = call(
-                round_body, wide, [upper, seen, total, total_log, before, before_log]
-            )
+            body = round_body if carry else first_body
+            message, total, total_log, *carry = call(body, wide, [upper, seen, total, total_log] + carry)
         distance *= 2
     intra, q_all = call(
         query_body,
@@ -336,25 +347,23 @@
         flops=8_000_000,
     )
     other = [swap(g, "tp", 1) for g in got]
-    steps = [0, 7] + [s + core for s in (1, 3, 5)] + [s + 1 - core for s in (1, 3, 5)]
-    seat = jnp.stack([jnp.asarray(v, jnp.int32) for v in [place, core] + [place ^ s for s in steps[1:]]])
     keys = [own, last] + got + other
     mla_heads, logs = call(
         attend_body,
         [((rows, local * VDM), BF16), ((local, rows), F32)],
-        [seat, q_all, value_up] + keys,
+        [one(place), one(core), q_all, value_up] + keys,
         flops=12_000_000,
         scratch=[pltpu.VMEM((len(keys), local * rows, rows), F32)],
     )
     ret_heads, near = call(
         heads_body,
         [((rows, heads * VD), BF16), ((rows, columns), BF16)],
-        [upper, seen, before, before_log, rq, col, intra, ret_gain[None], mla_heads, ret_out, mla_out],
+        [upper, seen] + carry + [rq, col, intra, ret_gain[None], mla_heads, ret_out, mla_out],
     )
     mine, theirs = call(
         merge_body,
         [((rows // 2, 2 * columns), BF16), ((rows // 2, 2 * columns), BF16)],
-        [jnp.stack([core, side]).astype(jnp.int32), near, ret_heads, mla_heads, far_ret, far_mla],
+        [one(core), one(side), near, ret_heads, mla_heads, far_ret, far_mla],
     )
     mixed = (mine.astype(F32) + swap(theirs, "tp", 1).astype(F32)).astype(BF16)
     return mixed[:, None, :], logs[None]

time: 59.4 us -> 57.6 us (0.970)
  Pallas kernels: 22.5 us -> 9.71 us
  local copies, waits for them, and re-layouts: 6.7 us -> 18.8 us
  other arithmetic: 2.91 us -> 0.78 us
  waiting for transfers between devices: 11.1 us -> 11.7 us
    unnamed x27 -> x66, local copies, waits for them, and re-layouts: 4.69 us -> 18.8 us
    pallas_call x8, Pallas kernels: 22.5 us -> 9.71 us  [call(): pl.pallas_call(body, out_shape=shapes, in_specs=specs, out_specs=[pl.Bloc...]
    broadcast_in_dim x2 -> x0, local copies, waits for them, and re-layouts: 1.34 us -> none  [with_kernels(): before, before_log = (jnp.zeros((big, VD), F32), jnp.zeros((16, VD), F32))]
    broadcast_in_dim x1, other arithmetic: 1.72 us -> 0.77 us  [with_kernels(): return (mixed[:, None, :], logs[None])]
    another operation x1 -> x0, local copies, waits for them, and re-layouts: 0.67 us -> none  [with_kernels(): jnp.stack([jnp.asarray(v, jnp.int32) for v in [place, core] + [place ^ s...]
    another operation x1 -> x0, other arithmetic: 0.67 us -> none  [with_kernels(): jnp.stack([core, side]).astype(jnp.int32)]
  transfers between devices with their start and end apart: 13 -> 13, of which waited for: 6 -> 5; matrix products, arithmetic and copies ran while one was open for 8% -> 2% of each run, Pallas kernels for 33% -> 16%
where the time goes in v1:
time: 57.6 us; the launch traced here: 56.8 us
  local copies, waits for them, and re-layouts  18.8 us (33%)
  starting transfers between devices  14.8 us (26%)
  waiting for transfers between devices  11.7 us (20%)
  Pallas kernels  9.71 us (17%)
  between operations  0.87 us (2%)
  other arithmetic  0.78 us (1%)
    unnamed x66, local copies, waits for them, and re-layouts  18.8 us
    ppermute x10, starting transfers between devices, swap(): return lax.ppermute(x, axis, [(i, i ^ distance) for i in range(size)])  10.4 us
    pallas_call x8, Pallas kernels, call(): pl.pallas_call(body, out_shape=shapes, in_specs=specs, out_specs=[pl.Bloc...  9.71 us
    ppermute x3, waiting for transfers between devices, with_kernels(): got.append(lax.ppermute(own, ('sp', 'tp'), perm))  6.11 us
    ppermute x10, waiting for transfers between devices, swap(): return lax.ppermute(x, axis, [(i, i ^ distance) for i in range(size)])  5.63 us
    ppermute x3, starting transfers between devices, with_kernels(): got.append(lax.ppermute(own, ('sp', 'tp'), perm))  4.44 us
  transfers between devices with their start and end apart: 13, of which 5 were waited for; matrix products, arithmetic and copies ran while one was open for 2% of the time, Pallas kernels for 16%

profile of v1, /device:TPU:0, one launch (start us, length us, event | category | flops | bytes accessed | tf_op | source)
XLA Modules:
  0.0 56.8 jit_solution(4065153585759932274)
XLA Ops:
  0.6 3.0 %collective-permute-start.10 = (bf16[512,1024]{1,0:T(8,128)(2,1)}, bf16[512,1024]{1,0:T(8,128)(2,1)S(1)}, u32[]{:S(2)}, u32[]{:S(2)}) collective-permute-start(bf16[512,1024]{1,0:T(8,128)(2,1)} %ret_w.1), channel_id=1, source_target_pairs={{0,2},{2,0},{1,3},{3,1},{4,6},{6,4},{5,7},{7,5},{8,10},{10,8},{9,1... | collective-permute-start | bytes 3145736 | tf_op jit(solution)/shard_map/ppermute | solution.py:20
  3.8 0.8 %copy.14 = bf16[128,1,64]{2,0,1:T(8,128)(2,1)S(1)} copy(bf16[128,1,64]{0,2,1:T(8,128)(2,1)} %param.19) | data formatting | bytes 32768 | tf_op args[7]
  4.6 0.8 %copy-done.21 = bf16[128,1,256]{2,0,1:T(8,128)(2,1)S(1)} copy-done((bf16[128,1,256]{2,0,1:T(8,128)(2,1)S(1)}, bf16[128,1,256]{2,0,1:T(8,128)(2,1)}, u32[]{:S(2)}) %copy-start.21) | copy-done | bytes 65560
  5.4 1.1 %shard_map.131 = (bf16[128,384]{1,0:T(8,128)(2,1)}, f32[128,128]{1,0:T(8,128)S(1)}, f32[128,128]{1,0:T(8,128)S(1)}) custom-call(s32[1]{0:T(128)} %bitcast.9.place, f32[1,128]{1,0:T(1,128)S(1)} %fusion.5.inverse, bf16[128,256]{1,0:T(8,128)(2,1)S(1)} %bitcast.22, bf16[128,64]{1,0:T(8,128)(2,1)S(1)} %bitcast.21), custom_call_target="tpu_custom_call" | custom-call | flops 2000000 | bytes 1000000 | tf_op jit(solution)/shard_map/pallas_call | solution.py:95
  7.2 0.8 %copy-done.22 = bf16[128,1,256]{2,0,1:T(8,128)(2,1)S(1)} copy-done((bf16[128,1,256]{2,0,1:T(8,128)(2,1)S(1)}, bf16[128,1,256]{2,0,1:T(8,128)(2,1)}, u32[]{:S(2)}) %copy-start.22) | copy-done | bytes 65560
  8.1 0.8 %copy-done.23 = bf16[128,1,256]{2,0,1:T(8,128)(2,1)S(1)} copy-done((bf16[128,1,256]{2,0,1:T(8,128)(2,1)S(1)}, bf16[128,1,256]{2,0,1:T(8,128)(2,1)}, u32[]{:S(2)}) %copy-start.23) | copy-done | bytes 65560
  11.9 2.0 %collective-permute-start = (bf16[272,256]{1,0:T(8,128)(2,1)S(1)}, bf16[272,256]{1,0:T(8,128)(2,1)S(1)}, u32[]{:S(2)}, u32[]{:S(2)}) collective-permute-start(bf16[272,256]{1,0:T(8,128)(2,1)S(1)} %get-tuple-element.30), channel_id=1, source_target_pairs={{0,4},{4,0},{8,12},{12,8},{16,20},{20,16},{24,28},{28,24},{1,5},{5... | collective-permute-start | bytes 417800 | tf_op jit(solution)/shard_map/ppermute | solution.py:20
  13.9 3.2 %collective-permute-done.seen = bf16[272,256]{1,0:T(8,128)(2,1)S(1)} collective-permute-done((bf16[272,256]{1,0:T(8,128)(2,1)S(1)}, bf16[272,256]{1,0:T(8,128)(2,1)S(1)}, u32[]{:S(2)}, u32[]{:S(2)}) %collective-permute-start) | collective-permute-done | bytes 139296 | tf_op jit(solution)/shard_map/ppermute | solution.py:20
  17.3 0.7 %copy-done.10 = f32[256,256]{1,0:T(8,128)} copy-done((f32[256,256]{1,0:T(8,128)}, f32[256,256]{1,0:T(8,128)S(1)}, u32[]{:S(2)}) %copy-start.10) | copy-done | bytes 262168
  19.2 2.0 %collective-permute-start.1 = (bf16[272,256]{1,0:T(8,128)(2,1)S(1)}, bf16[272,256]{1,0:T(8,128)(2,1)S(1)}, u32[]{:S(2)}, u32[]{:S(2)}) collective-permute-start(bf16[272,256]{1,0:T(8,128)(2,1)S(1)} %get-tuple-element.33), channel_id=1, source_target_pairs={{0,8},{4,12},{8,0},{12,4},{16,24},{20,28},{24,16},{28,20},{1,9},{5... | collective-permute-start | bytes 417800 | tf_op jit(solution)/shard_map/ppermute | solution.py:20
  21.1 3.5 %collective-permute-start.6 = (bf16[128,384]{1,0:T(8,128)(2,1)}, bf16[128,384]{1,0:T(8,128)(2,1)S(1)}, u32[]{:S(2)}, u32[]{:S(2)}) collective-permute-start(bf16[128,384]{1,0:T(8,128)(2,1)} %get-tuple-element.47.rest_0_), channel_id=1, source_target_pairs={{0,20},{1,25},{4,16},{5,29},{8,28},{9,17},{12,24},{13,21},{16,4},{... | collective-permute-start | bytes 294920 | tf_op jit(solution)/shard_map/ppermute | solution.py:325
  25.1 5.4 %collective-permute-done.6.rest_4_ = bf16[128,384]{1,0:T(8,128)(2,1)S(1)} collective-permute-done((bf16[128,384]{1,0:T(8,128)(2,1)}, bf16[128,384]{1,0:T(8,128)(2,1)S(1)}, u32[]{:S(2)}, u32[]{:S(2)}) %collective-permute-start.6) | collective-permute-done | bytes 98336 | tf_op jit(solution)/shard_map/ppermute | solution.py:325
  30.9 0.7 %collective-permute-done.5.rest_3_ = bf16[128,384]{1,0:T(8,128)(2,1)} collective-permute-done((bf16[128,384]{1,0:T(8,128)(2,1)}, bf16[128,384]{1,0:T(8,128)(2,1)}, u32[]{:S(2)}, u32[]{:S(2)}) %collective-permute-start.5) | collective-permute-done | bytes 98336 | tf_op jit(solution)/shard_map/ppermute | solution.py:325
  31.7 2.8 %collective-permute-start.3 = (bf16[128,384]{1,0:T(8,128)(2,1)}, bf16[128,384]{1,0:T(8,128)(2,1)}, u32[]{:S(2)}, u32[]{:S(2)}) collective-permute-start(bf16[128,384]{1,0:T(8,128)(2,1)} %get-tuple-element.47.rest_0_), channel_id=1, source_target_pairs={{0,28},{4,24},{8,20},{12,16},{16,12},{20,8},{24,4},{28,0},{1,29},{... | collective-permute-start | bytes 294920 | tf_op jit(solution)/shard_map/ppermute | solution.py:20
  34.4 0.9 %copy-done.11 = f32[256,256]{1,0:T(8,128)S(1)} copy-done((f32[256,256]{1,0:T(8,128)S(1)}, f32[256,256]{1,0:T(8,128)}, u32[]{:S(2)}) %copy-start.11) | copy-done | bytes 262168
  35.4 0.7 %copy-done.25 = f32[16,256]{1,0:T(8,128)S(1)} copy-done((f32[16,256]{1,0:T(8,128)S(1)}, f32[16,256]{1,0:T(8,128)}, u32[]{:S(2)}) %copy-start.25) | copy-done | bytes 16408
  36.1 0.7 %copy-done.27 = f32[16,256]{1,0:T(8,128)S(1)} copy-done((f32[16,256]{1,0:T(8,128)S(1)}, f32[16,256]{1,0:T(8,128)}, u32[]{:S(2)}) %copy-start.27) | copy-done | bytes 16408
  36.8 0.9 %shard_map.134 = (bf16[272,256]{1,0:T(8,128)(2,1)}, f32[256,256]{1,0:T(8,128)}, f32[16,256]{1,0:T(8,128)}, f32[256,256]{1,0:T(8,128)S(1)}, f32[16,256]{1,0:T(8,128)S(1)}) custom-call(s32[1]{0:T(128)} %bitcast.3.upper, bf16[272,256]{1,0:T(8,128)(2,1)S(1)} %collective-permute-done.1.seen, f32[256,256]{1,0:T(8,128)S(1)} %get-tuple-element.34.total, ...), custom_call_target="tpu_custom_call" | custom-call | flops 2000000 | bytes 1000000 | tf_op jit(solution)/shard_map/pallas_call | solution.py:95
  37.8 1.5 %collective-permute-done.3.rest_1_ = bf16[128,384]{1,0:T(8,128)(2,1)} collective-permute-done((bf16[128,384]{1,0:T(8,128)(2,1)}, bf16[128,384]{1,0:T(8,128)(2,1)}, u32[]{:S(2)}, u32[]{:S(2)}) %collective-permute-start.3) | collective-permute-done | bytes 98336 | tf_op jit(solution)/shard_map/ppermute | solution.py:20
  39.8 0.9 %copy-done.6 = bf16[128,256]{1,0:T(8,128)(2,1)S(1)} copy-done((bf16[128,256]{1,0:T(8,128)(2,1)S(1)}, bf16[128,256]{1,0:T(8,128)(2,1)}, u32[]{:S(2)}) %copy-start.6) | copy-done | bytes 65560
  40.7 0.8 %copy-done.8 = f32[128,8]{1,0:T(8,128)S(1)} copy-done((f32[128,8]{1,0:T(8,128)S(1)}, f32[128,8]{1,0:T(8,128)}, u32[]{:S(2)}) %copy-start.8) | copy-done | bytes 4120
  41.6 0.8 %copy-done.13 = f32[128,128]{1,0:T(8,128)S(1)} copy-done((f32[128,128]{1,0:T(8,128)S(1)}, f32[128,128]{1,0:T(8,128)}, u32[]{:S(2)}) %copy-start.13) | copy-done | bytes 65560
  42.4 0.8 %copy-done.15 = f32[128,128]{1,0:T(8,128)S(1)} copy-done((f32[128,128]{1,0:T(8,128)S(1)}, f32[128,128]{1,0:T(8,128)}, u32[]{:S(2)}) %copy-start.15) | copy-done | bytes 65560
  43.2 0.9 %copy-done.16 = bf16[128,1,768]{2,0,1:T(8,128)(2,1)S(1)} copy-done((bf16[128,1,768]{2,0,1:T(8,128)(2,1)S(1)}, bf16[128,1,768]{2,0,1:T(8,128)(2,1)}, u32[]{:S(2)}) %copy-start.16) | copy-done | bytes 196632
  44.2 0.8 %copy-done.20 = bf16[128,256]{1,0:T(8,128)(2,1)S(1)} copy-done((bf16[128,256]{1,0:T(8,128)(2,1)S(1)}, bf16[128,256]{1,0:T(8,128)(2,1)}, u32[]{:S(2)}) %copy-start.20) | copy-done | bytes 65560
  45.0 0.7 %copy-done.29 = f32[8,128]{1,0:T(8,128)S(1)} copy-done((f32[8,128]{1,0:T(8,128)S(1)}, f32[8,128]{1,0:T(8,128)}, u32[]{:S(2)}) %copy-start.29) | copy-done | bytes 4120
  45.7 0.8 %shard_map.135 = (f32[128,512]{1,0:T(8,128)S(1)}, bf16[512,384]{1,0:T(8,128)(2,1)S(1)}) custom-call(s32[1]{0:T(128)} %bitcast.core, bf16[128,256]{1,0:T(8,128)(2,1)S(1)} %copy-done.6, bf16[128,256]{1,0:T(8,128)(2,1)S(1)} %copy-done.20, bf16[128,512]{1,0:T(8,128)(2,1)S(1)} %bitcast.19, f32[128,8]{1,0:T(8,128)S(1)} %copy-done.8, f32[8,128]{1,0:T(8,128)S(1)} %copy-done.29, ...), custom_call_target="tpu_custom_call" | custom-call | flops 8000000 | bytes 1000000 | tf_op jit(solution)/shard_map/pallas_call | solution.py:95
  46.5 1.0 %copy-done.18 = bf16[128,384]{1,0:T(8,128)(2,1)S(1)} copy-done((bf16[128,384]{1,0:T(8,128)(2,1)S(1)}, bf16[128,384]{1,0:T(8,128)(2,1)}, u32[]{:S(2)}) %copy-start.18) | copy-done | bytes 98328
  47.5 4.2 %shard_map.136 = (bf16[128,512]{1,0:T(8,128)(2,1)S(1)}, f32[4,128]{1,0:T(4,128)S(1)}) custom-call(s32[1]{0:T(128)} %bitcast.9.place, s32[1]{0:T(128)} %bitcast.core, bf16[512,384]{1,0:T(8,128)(2,1)S(1)} %get-tuple-element.46.q_all, bf16[256,1024]{1,0:T(8,128)(2,1)S(1)} %copy-done.2, bf16[128,384]{1,0:T(8,128)(2,1)} %get-tuple-element.47.rest_0_, ...), custom_call_target="tpu_custom_call" | custom-call | flops 12000000 | bytes 1000000 | tf_op jit(solution)/shard_map/pallas_call | solution.py:95
  52.4 1.5 %shard_map.137 = (bf16[128,512]{1,0:T(8,128)(2,1)S(1)}, bf16[128,1024]{1,0:T(8,128)(2,1)S(1)}) custom-call(s32[1]{0:T(128)} %bitcast.2.upper, bf16[272,256]{1,0:T(8,128)(2,1)} %collective-permute-done.2.seen, f32[256,256]{1,0:T(8,128)S(1)} %get-tuple-element.39.before, f32[16,256]{1,0:T(8,128)S(1)} %get-tuple-element.40.before_log, ...), custom_call_target="tpu_custom_call" | custom-call | flops 2000000 | bytes 1000000 | tf_op jit(solution)/shard_map/pallas_call | solution.py:95
  55.1 0.9 %collective-permute-done.12 = bf16[64,2048]{1,0:T(8,128)(2,1)S(1)} collective-permute-done((bf16[64,2048]{1,0:T(8,128)(2,1)S(1)}, bf16[64,2048]{1,0:T(8,128)(2,1)S(1)}, u32[]{:S(2)}, u32[]{:S(2)}) %collective-permute-start.12) | collective-permute-done | bytes 262176 | tf_op jit(solution)/shard_map/ppermute | solution.py:20
  56.0 0.8 %fusion = bf16[64,1,2048]{2,0,1:T(8,128)(2,1)} fusion(bf16[64,2048]{1,0:T(8,128)(2,1)S(1)} %collective-permute-done.12, bf16[64,2048]{1,0:T(8,128)(2,1)S(1)} %get-tuple-element.51), kind=kLoop, calls=%fused_computation.1 | loop fusion | flops 524288 | bytes 786432 | tf_op jit(solution)/shard_map/broadcast_in_dim | solution.py:369
  (70 shorter events, 8.4 us)
Async XLA Ops:
  0.6 5.9 %copy-start.3 = (bf16[128,1,512]{2,0,1:T(8,128)(2,1)S(1)}, bf16[128,1,512]{2,0,1:T(8,128)(2,1)}, u32[]{:S(2)}) copy-start(bf16[128,1,512]{2,0,1:T(8,128)(2,1)} %param.14) | copy-start | bytes 393220
  0.6 53.3 %collective-permute-start.10 = (bf16[512,1024]{1,0:T(8,128)(2,1)}, bf16[512,1024]{1,0:T(8,128)(2,1)S(1)}, u32[]{:S(2)}, u32[]{:S(2)}) collective-permute-start(bf16[512,1024]{1,0:T(8,128)(2,1)} %ret_w.1), channel_id=1, source_target_pairs={{0,2},{2,0},{1,3},{3,1},{4,6},{6,4},{5,7},{7,5},{8,10},{10,8},{9,1... | collective-permute-start | bytes 3145736 | tf_op jit(solution)/shard_map/ppermute | solution.py:20
  3.7 50.2 %collective-permute-start.11 = (bf16[512,1024]{1,0:T(8,128)(2,1)}, bf16[512,1024]{1,0:T(8,128)(2,1)S(1)}, u32[]{:S(2)}, u32[]{:S(2)}) collective-permute-start(bf16[512,1024]{1,0:T(8,128)(2,1)} %mla_w.1), channel_id=1, source_target_pairs={{0,2},{2,0},{1,3},{3,1},{4,6},{6,4},{5,7},{7,5},{8,10},{10,8},{9,1... | collective-permute-start | bytes 3145736 | tf_op jit(solution)/shard_map/ppermute | solution.py:20
  4.6 0.8 %copy-start.21 = (bf16[128,1,256]{2,0,1:T(8,128)(2,1)S(1)}, bf16[128,1,256]{2,0,1:T(8,128)(2,1)}, u32[]{:S(2)}) copy-start(bf16[128,1,256]{2,0,1:T(8,128)(2,1)} %param.18) | copy-start | bytes 196612
  6.5 2.9 %copy-start.12 = (f32[128,128]{1,0:T(8,128)}, f32[128,128]{1,0:T(8,128)S(1)}, u32[]{:S(2)}) copy-start(f32[128,128]{1,0:T(8,128)S(1)} %get-tuple-element.28.cos) | copy-start | bytes 196612
  6.5 2.9 %copy-start.14 = (f32[128,128]{1,0:T(8,128)}, f32[128,128]{1,0:T(8,128)S(1)}, u32[]{:S(2)}) copy-start(f32[128,128]{1,0:T(8,128)S(1)} %get-tuple-element.29.sin) | copy-start | bytes 196612
  7.2 0.8 %copy-start.22 = (bf16[128,1,256]{2,0,1:T(8,128)(2,1)S(1)}, bf16[128,1,256]{2,0,1:T(8,128)(2,1)}, u32[]{:S(2)}) copy-start(bf16[128,1,256]{2,0,1:T(8,128)(2,1)} %param.12) | copy-start | bytes 196612
  8.1 0.8 %copy-start.23 = (bf16[128,1,256]{2,0,1:T(8,128)(2,1)S(1)}, bf16[128,1,256]{2,0,1:T(8,128)(2,1)}, u32[]{:S(2)}) copy-start(bf16[128,1,256]{2,0,1:T(8,128)(2,1)} %param.13) | copy-start | bytes 196612
  11.9 5.1 %collective-permute-start = (bf16[272,256]{1,0:T(8,128)(2,1)S(1)}, bf16[272,256]{1,0:T(8,128)(2,1)S(1)}, u32[]{:S(2)}, u32[]{:S(2)}) collective-permute-start(bf16[272,256]{1,0:T(8,128)(2,1)S(1)} %get-tuple-element.30), channel_id=1, source_target_pairs={{0,4},{4,0},{8,12},{12,8},{16,20},{20,16},{24,28},{28,24},{1,5},{5... | collective-permute-start | bytes 417800 | tf_op jit(solution)/shard_map/ppermute | solution.py:20
  17.1 22.8 %copy-start.4 = (bf16[256,1024]{1,0:T(8,128)(2,1)S(1)}, bf16[256,1024]{1,0:T(8,128)(2,1)}, u32[]{:S(2)}) copy-start(bf16[256,1024]{1,0:T(8,128)(2,1)} %key_up.1) | copy-start | bytes 1572868
  19.2 15.3 %collective-permute-start.1 = (bf16[272,256]{1,0:T(8,128)(2,1)S(1)}, bf16[272,256]{1,0:T(8,128)(2,1)S(1)}, u32[]{:S(2)}, u32[]{:S(2)}) collective-permute-start(bf16[272,256]{1,0:T(8,128)(2,1)S(1)} %get-tuple-element.33), channel_id=1, source_target_pairs={{0,8},{4,12},{8,0},{12,4},{16,24},{20,28},{24,16},{28,20},{1,9},{5... | collective-permute-start | bytes 417800 | tf_op jit(solution)/shard_map/ppermute | solution.py:20
  21.1 9.3 %collective-permute-start.6 = (bf16[128,384]{1,0:T(8,128)(2,1)}, bf16[128,384]{1,0:T(8,128)(2,1)S(1)}, u32[]{:S(2)}, u32[]{:S(2)}) collective-permute-start(bf16[128,384]{1,0:T(8,128)(2,1)} %get-tuple-element.47.rest_0_), channel_id=1, source_target_pairs={{0,20},{1,25},{4,16},{5,29},{8,28},{9,17},{12,24},{13,21},{16,4},{... | collective-permute-start | bytes 294920 | tf_op jit(solution)/shard_map/ppermute | solution.py:325
  24.7 7.0 %collective-permute-start.5 = (bf16[128,384]{1,0:T(8,128)(2,1)}, bf16[128,384]{1,0:T(8,128)(2,1)}, u32[]{:S(2)}, u32[]{:S(2)}) collective-permute-start(bf16[128,384]{1,0:T(8,128)(2,1)} %get-tuple-element.47.rest_0_), channel_id=1, source_target_pairs={{0,12},{1,17},{4,8},{5,21},{8,4},{9,25},{12,0},{13,29},{16,28},{17... | collective-permute-start | bytes 294920 | tf_op jit(solution)/shard_map/ppermute | solution.py:325
  30.4 7.3 %copy-start.17 = (bf16[128,384]{1,0:T(8,128)(2,1)}, bf16[128,384]{1,0:T(8,128)(2,1)S(1)}, u32[]{:S(2)}) copy-start(bf16[128,384]{1,0:T(8,128)(2,1)S(1)} %collective-permute-done.6.rest_4_) | copy-start | bytes 294916
  30.4 7.3 %collective-permute-start.4 = (bf16[128,384]{1,0:T(8,128)(2,1)}, bf16[128,384]{1,0:T(8,128)(2,1)}, u32[]{:S(2)}, u32[]{:S(2)}) collective-permute-start(bf16[128,384]{1,0:T(8,128)(2,1)} %get-tuple-element.47.rest_0_), channel_id=1, source_target_pairs={{0,4},{1,9},{4,0},{5,13},{8,12},{9,1},{12,8},{13,5},{16,20},{17,25... | collective-permute-start | bytes 294920 | tf_op jit(solution)/shard_map/ppermute | solution.py:325
  31.7 7.6 %collective-permute-start.3 = (bf16[128,384]{1,0:T(8,128)(2,1)}, bf16[128,384]{1,0:T(8,128)(2,1)}, u32[]{:S(2)}, u32[]{:S(2)}) collective-permute-start(bf16[128,384]{1,0:T(8,128)(2,1)} %get-tuple-element.47.rest_0_), channel_id=1, source_target_pairs={{0,28},{4,24},{8,20},{12,16},{16,12},{20,8},{24,4},{28,0},{1,29},{... | collective-permute-start | bytes 294920 | tf_op jit(solution)/shard_map/ppermute | solution.py:20
  34.4 4.9 %collective-permute-start.9 = (bf16[128,384]{1,0:T(8,128)(2,1)S(1)}, bf16[128,384]{1,0:T(8,128)(2,1)}, u32[]{:S(2)}, u32[]{:S(2)}) collective-permute-start(bf16[128,384]{1,0:T(8,128)(2,1)S(1)} %collective-permute-done.6.rest_4_), channel_id=1, source_target_pairs={{0,1},{1,0},{2,3},{3,2},{4,5},{5,4},{6,7},{7,6},{8,9},{9,8},{10,11... | collective-permute-start | bytes 294920 | tf_op jit(solution)/shard_map/ppermute | solution.py:20
  34.4 1.0 %copy-start.11 = (f32[256,256]{1,0:T(8,128)S(1)}, f32[256,256]{1,0:T(8,128)}, u32[]{:S(2)}) copy-start(f32[256,256]{1,0:T(8,128)} %copy-done.10) | copy-start | bytes 786436
  37.8 13.9 %collective-permute-start.2 = (bf16[272,256]{1,0:T(8,128)(2,1)}, bf16[272,256]{1,0:T(8,128)(2,1)}, u32[]{:S(2)}, u32[]{:S(2)}) collective-permute-start(bf16[272,256]{1,0:T(8,128)(2,1)} %get-tuple-element.38), channel_id=1, source_target_pairs={{0,16},{4,20},{8,24},{12,28},{16,0},{20,4},{24,8},{28,12},{1,17},{... | collective-permute-start | bytes 417800 | tf_op jit(solution)/shard_map/ppermute | solution.py:20
  39.3 7.2 %collective-permute-start.8 = (bf16[128,384]{1,0:T(8,128)(2,1)}, bf16[128,384]{1,0:T(8,128)(2,1)}, u32[]{:S(2)}, u32[]{:S(2)}) collective-permute-start(bf16[128,384]{1,0:T(8,128)(2,1)} %collective-permute-done.5.rest_3_), channel_id=1, source_target_pairs={{0,1},{1,0},{2,3},{3,2},{4,5},{5,4},{6,7},{7,6},{8,9},{9,8},{10,11... | collective-permute-start | bytes 294920 | tf_op jit(solution)/shard_map/ppermute | solution.py:20
  39.3 7.2 %collective-permute-start.7 = (bf16[128,384]{1,0:T(8,128)(2,1)}, bf16[128,384]{1,0:T(8,128)(2,1)}, u32[]{:S(2)}, u32[]{:S(2)}) collective-permute-start(bf16[128,384]{1,0:T(8,128)(2,1)} %collective-permute-done.4.rest_2_), channel_id=1, source_target_pairs={{0,1},{1,0},{2,3},{3,2},{4,5},{5,4},{6,7},{7,6},{8,9},{9,8},{10,11... | collective-permute-start | bytes 294920 | tf_op jit(solution)/shard_map/ppermute | solution.py:20
  39.8 6.7 %copy-start.2 = (bf16[256,1024]{1,0:T(8,128)(2,1)S(1)}, bf16[256,1024]{1,0:T(8,128)(2,1)}, u32[]{:S(2)}) copy-start(bf16[256,1024]{1,0:T(8,128)(2,1)} %value_up.1) | copy-start | bytes 1572868
  39.8 0.9 %copy-start.6 = (bf16[128,256]{1,0:T(8,128)(2,1)S(1)}, bf16[128,256]{1,0:T(8,128)(2,1)}, u32[]{:S(2)}) copy-start(bf16[128,256]{1,0:T(8,128)(2,1)} %copy-done.5) | copy-start | bytes 196612
  40.7 0.8 %copy-start.8 = (f32[128,8]{1,0:T(8,128)S(1)}, f32[128,8]{1,0:T(8,128)}, u32[]{:S(2)}) copy-start(f32[128,8]{1,0:T(8,128)} %copy-done.7) | copy-start | bytes 12292
  41.6 0.8 %copy-start.13 = (f32[128,128]{1,0:T(8,128)S(1)}, f32[128,128]{1,0:T(8,128)}, u32[]{:S(2)}) copy-start(f32[128,128]{1,0:T(8,128)} %copy-done.12) | copy-start | bytes 196612
  43.2 0.9 %copy-start.16 = (bf16[128,1,768]{2,0,1:T(8,128)(2,1)S(1)}, bf16[128,1,768]{2,0,1:T(8,128)(2,1)}, u32[]{:S(2)}) copy-start(bf16[128,1,768]{2,0,1:T(8,128)(2,1)} %param.17) | copy-start | bytes 589828
  44.2 0.8 %copy-start.20 = (bf16[128,256]{1,0:T(8,128)(2,1)S(1)}, bf16[128,256]{1,0:T(8,128)(2,1)}, u32[]{:S(2)}) copy-start(bf16[128,256]{1,0:T(8,128)(2,1)} %copy-done.19) | copy-start | bytes 196612
  45.7 6.0 %copy-start.1 = (bf16[512,1024]{1,0:T(8,128)(2,1)S(1)}, bf16[512,1024]{1,0:T(8,128)(2,1)}, u32[]{:S(2)}) copy-start(bf16[512,1024]{1,0:T(8,128)(2,1)} %mla_w.1) | copy-start | bytes 3145732
  46.5 5.2 %copy-start = (bf16[512,1024]{1,0:T(8,128)(2,1)S(1)}, bf16[512,1024]{1,0:T(8,128)(2,1)}, u32[]{:S(2)}) copy-start(bf16[512,1024]{1,0:T(8,128)(2,1)} %ret_w.1) | copy-start | bytes 3145732
  46.5 1.0 %copy-start.18 = (bf16[128,384]{1,0:T(8,128)(2,1)S(1)}, bf16[128,384]{1,0:T(8,128)(2,1)}, u32[]{:S(2)}) copy-start(bf16[128,384]{1,0:T(8,128)(2,1)} %copy-done.17) | copy-start | bytes 294916
  47.5 4.2 %copy-start.9 = (f32[128,8]{1,0:T(8,128)S(1)}, f32[128,8]{1,0:T(8,128)}, u32[]{:S(2)}) copy-start(f32[128,8]{1,0:T(8,128)} %copy-done.7) | copy-start | bytes 12292
  54.4 1.6 %collective-permute-start.12 = (bf16[64,2048]{1,0:T(8,128)(2,1)S(1)}, bf16[64,2048]{1,0:T(8,128)(2,1)S(1)}, u32[]{:S(2)}, u32[]{:S(2)}) collective-permute-start(bf16[64,2048]{1,0:T(8,128)(2,1)S(1)} %get-tuple-element.52), channel_id=1, source_target_pairs={{0,1},{1,0},{2,3},{3,2},{4,5},{5,4},{6,7},{7,6},{8,9},{9,8},{10,11... | collective-permute-start | bytes 786440 | tf_op jit(solution)/shard_map/ppermute | solution.py:20
  (13 other events, 8.7 us)
